TPU v7x, 32 devices: a whole 2x2x4 slice. The times are simulated.
32 devices in a mesh: ep: 8 (over z, core), tp: 4 (over y, x).
Axes of the slice: x: 2, y: 2, z: 4, core: 2. Of those that a mesh axis runs over, the one named last changes fastest.
Arguments:
- receptance: bfloat16 [2048, 2048], P('ep', 'tp'), may hold values from -6 to 6
- key_tensor: bfloat16 [2048, 2048], P('ep', 'tp'), may hold values from -6 to 6
- value_tensor: bfloat16 [2048, 2048], P('ep', 'tp'), may hold values from -6 to 6
- decay_data_input: bfloat16 [2048, 2048], P('ep', 'tp'), may hold values from -4 to 4
- correction_rate_input: bfloat16 [2048, 2048], P('ep', 'tp'), may hold values from -16 to 6
- mixer_output_gate: bfloat16 [2048, 2048], P('ep', 'tp'), may hold values from -6 to 6
- decay_channel_offset: float32 [2048], P('tp'), may hold values from -16 to -3
- head_norm_gain: float32 [2048], P('tp'), may hold values from 0.1 to 1.9
- self_key_weight: float32 [2048], P('tp'), may hold values from -2 to 2
- mixer_output_weight: bfloat16 [2048, 2048], P('tp'), may hold values from -0.125 to 0.125
- second_batch_rows: bfloat16 [1024, 2048], P('ep'), may hold values from -6 to 6
- routed_expert_index: int32 [1024, 4], P('ep'), may hold values from 0 to 7, all different within a row; in each aligned block of 128 rows (0 to 127, 128 to 255, ...) at most 96 rows name the same one
- routing_output_weight: float32 [1024, 4], P('ep'), may hold values from 0.1 to 1
- expert_norm_gain: float32 [2048], replicated, may hold values from 0.1 to 1.9
- expert_gate_weight: bfloat16 [8, 1024, 2048], P('ep', 'tp'), may hold values from -0.125 to 0.125
- expert_up_weight: bfloat16 [8, 1024, 2048], P('ep', 'tp'), may hold values from -0.125 to 0.125
- expert_down_weight: bfloat16 [8, 1024, 2048], P('ep', None, 'tp'), may hold values from -0.1875 to 0.1875
- common_expert_gate: bfloat16 [1024, 2048], P('tp'), may hold values from -0.125 to 0.125
- common_expert_up: bfloat16 [1024, 2048], P('tp'), may hold values from -0.125 to 0.125
- common_expert_down: bfloat16 [1024, 2048], P(None, 'tp'), may hold values from -0.1875 to 0.1875
Outputs:
- token_mixer_output: bfloat16 [2048, 2048], P(('ep', 'tp'))
- expert_out: bfloat16 [1024, 2048], P('ep', 'tp')
Inputs may be any that keep to these rules, and one draw needn't show every extreme that they name: `routed_expert_index`: each row names 4 different experts. Within the rows of one index of ep no expert is named by more than 96 rows, and that bound is met in some index's rows.
All inputs are finite; a program needn't handle non-finite values.
Results may differ from a plain program's by a relative error of at most 0.017.
Values may be sent and summed in bfloat16 or wider, within the bound.
A program may use at most 128 MiB of HBM per device.

v0:
```python
import math
import jax
import jax.numpy as jnp
from jax import lax
from jax.sharding import PartitionSpec as P

HEAD_CHANNELS = 64
SPAN = 64
HIGHEST = lax.Precision.HIGHEST
PRECISION = lax.Precision.HIGH
NORM_FLOOR = 1.0


def head_view(matrix):
    return matrix.astype(jnp.float32).reshape(matrix.shape[0], -1, HEAD_CHANNELS)


def complete_head_outputs(
    state_readout,
    receptance_rows,
    key_row_block,
    value_row_block,
    head_norm_gain,
    self_key_weight,
    mixer_output_gate,
):
    mean_part = jnp.mean(state_readout, axis=-1, keepdims=True)
    spread = jnp.mean(jnp.square(state_readout - mean_part), axis=-1, keepdims=True)
    normalized_rows = (state_readout - mean_part) * lax.rsqrt(spread + NORM_FLOOR)
    sequence_length = state_readout.shape[0]
    normalized_rows = normalized_rows.reshape(sequence_length, -1) * head_norm_gain
    self_key_term = (
        jnp.sum(
            receptance_rows * key_row_block * self_key_weight.reshape(-1, HEAD_CHANNELS),
            axis=-1,
            keepdims=True,
        )
        * value_row_block
    )
    mixer_result = (
        normalized_rows + self_key_term.reshape(sequence_length, -1)
    ) * mixer_output_gate.astype(jnp.float32)
    return mixer_result.astype(jnp.bfloat16)


def product(spec, left, right):
    return jnp.einsum(spec, left, right, precision=PRECISION, preferred_element_type=jnp.float32)


def lower_inverse(strict, size):
    at = jnp.arange(size)
    row, column = (at[:, None], at[None, :])
    inverse = None
    block = 1
    while block < size:
        pair = (
            (row // (2 * block) == column // (2 * block))
            & (row // block % 2 == 1)
            & (column // block % 2 == 0)
        )
        below = jnp.where(pair, strict, 0.0)
        if inverse is None:
            inverse = jnp.eye(size, dtype=jnp.float32) - below
        else:
            inverse = inverse - product(
                "nhij,nhjk->nhik", product("nhij,nhjk->nhik", inverse, below), inverse
            )
        block *= 2
    return inverse


def mixer_part(
    receptance,
    key_tensor,
    value_tensor,
    decay_data_input,
    correction_rate_input,
    mixer_output_gate,
    decay_channel_offset,
    head_norm_gain,
    self_key_weight,
    mixer_output_weight,
):
    row_count, width = receptance.shape
    head_count = width // HEAD_CHANNELS
    span = min(SPAN, row_count)
    block_count = row_count // span
    receptance_rows = head_view(receptance)
    key_row_block = head_view(key_tensor)
    value_row_block = head_view(value_tensor)

    def by_block(matrix):
        return (
            matrix.astype(jnp.float32)
            .reshape(block_count, span, head_count, HEAD_CHANNELS)
            .transpose(0, 2, 1, 3)
        )

    step_log = -math.exp(-0.5) * jax.nn.sigmoid(
        decay_channel_offset + decay_data_input.astype(jnp.float32)
    )
    at = jnp.arange(span)
    reach = (at[:, None] >= at[None, :]).astype(jnp.float32)
    step_log = by_block(step_log)
    total_log = jnp.einsum("ts,nhsd->nhtd", reach, step_log, precision=HIGHEST)
    recept, keys, values = (by_block(receptance), by_block(key_tensor), by_block(value_tensor))
    units = keys * lax.rsqrt(jnp.sum(keys * keys, axis=-1, keepdims=True) + 1.0)
    corrections = units * jax.nn.sigmoid(by_block(correction_rate_input))
    grown = jnp.exp(-total_log)
    last_log = total_log[:, :, -1:, :]
    unit_in = units * jnp.exp(total_log - step_log)
    recept_in = recept * jnp.exp(total_log)
    tail = jnp.exp(last_log - total_log)
    scores = product(
        "nhtd,nhsd->nhts",
        jnp.concatenate([unit_in, recept_in], axis=2),
        jnp.concatenate([keys * grown, corrections * grown], axis=2),
    )
    before = at[:, None] > at[None, :]
    upto = at[:, None] >= at[None, :]
    unit_key = jnp.where(before, scores[:, :, :span, :span], 0.0)
    unit_fix = jnp.where(before, scores[:, :, :span, span:], 0.0)
    read_key = jnp.where(upto, scores[:, :, span:, :span], 0.0)
    read_fix = jnp.where(upto, scores[:, :, span:, span:], 0.0)
    inverse = lower_inverse(unit_fix, span)
    key_values = product("nhts,nhsd->nhtd", jnp.concatenate([unit_key, read_key], axis=2), values)
    solved = product(
        "nhts,nhsd->nhtd", inverse, jnp.concatenate([unit_in, key_values[:, :, :span]], axis=3)
    )
    reads = jnp.concatenate([recept_in, key_values[:, :, span:]], axis=3) - product(
        "nhts,nhsd->nhtd", read_fix, solved
    )
    eye_head = jnp.eye(HEAD_CHANNELS, dtype=jnp.float32)
    fresh = product("nhtj,nhti->nhji", keys * tail, values)
    moves = jnp.concatenate([eye_head * jnp.exp(last_log), fresh], axis=3) - product(
        "nhtj,nhti->nhji", corrections * tail, solved
    )
    whole = moves[0]
    for block in range(1, block_count):
        step = product("hij,hjk->hik", moves[block, :, :, :HEAD_CHANNELS], whole)
        whole = step + jnp.concatenate(
            [jnp.zeros_like(step[..., :HEAD_CHANNELS]), moves[block, :, :, HEAD_CHANNELS:]], axis=2
        )
    everything = lax.all_gather(whole.astype(jnp.bfloat16), "ep")
    mine = lax.axis_index("ep")
    state = jnp.zeros((head_count, HEAD_CHANNELS, HEAD_CHANNELS), jnp.float32)
    for k in range(lax.axis_size("ep") - 1):
        part = everything[k].astype(jnp.float32)
        new = product("hij,hjk->hik", part[..., :HEAD_CHANNELS], state)
        state = jnp.where(k < mine, new + part[..., HEAD_CHANNELS:], state)
    starts = [state]
    for block in range(block_count - 1):
        state = (
            product("hij,hjk->hik", moves[block, :, :, :HEAD_CHANNELS], state)
            + moves[block, :, :, HEAD_CHANNELS:]
        )
        starts.append(state)
    merged_output = reads[..., HEAD_CHANNELS:] + product(
        "nhtj,nhji->nhti", reads[..., :HEAD_CHANNELS], jnp.stack(starts)
    )
    merged_output = merged_output.transpose(0, 2, 1, 3).reshape(
        row_count, head_count, HEAD_CHANNELS
    )
    mixer_result = complete_head_outputs(
        merged_output,
        receptance_rows,
        key_row_block,
        value_row_block,
        head_norm_gain,
        self_key_weight,
        mixer_output_gate,
    )
    return lax.psum_scatter(
        jnp.dot(mixer_result, mixer_output_weight, preferred_element_type=jnp.float32).astype(
            jnp.bfloat16
        ),
        "tp",
        scatter_dimension=0,
        tiled=True,
    )


def activate(rows_in, gate_part, up_part):
    pre_gate = jnp.einsum("fd,rd->fr", gate_part, rows_in, preferred_element_type=jnp.float32)
    pre_up = jnp.einsum("fd,rd->fr", up_part, rows_in, preferred_element_type=jnp.float32)
    return (jax.nn.silu(pre_gate) * pre_up).astype(jnp.bfloat16)


def expert_entry(
    second_batch_rows,
    routed_expert_index,
    routing_output_weight,
    expert_norm_gain,
    common_expert_gate,
    common_expert_up,
):
    row_count, width = second_batch_rows.shape
    top_count = routed_expert_index.shape[1]
    peer_count = lax.axis_size("ep")
    slot_count = 3 * row_count * top_count // (2 * peer_count)
    widened = second_batch_rows.astype(jnp.float32)
    normalized_rows = (
        widened
        * lax.rsqrt(jnp.mean(widened * widened, axis=-1, keepdims=True) + NORM_FLOOR)
        * expert_norm_gain
    ).astype(jnp.bfloat16)
    flat_ids = routed_expert_index.reshape(-1)
    one_hot = (flat_ids[:, None] == jnp.arange(peer_count, dtype=jnp.int32)[None, :]).astype(
        jnp.int32
    )
    slot_rank = jnp.sum((jnp.cumsum(one_hot, axis=0) - 1) * one_hot, axis=1)
    target = flat_ids * slot_count + slot_rank
    owners = jnp.arange(row_count * top_count, dtype=jnp.int32) // top_count
    source_row = jnp.full((peer_count * slot_count,), row_count, jnp.int32).at[target].set(owners)
    padded = jnp.concatenate([normalized_rows, jnp.zeros((1, width), jnp.bfloat16)], axis=0)
    outgoing = jnp.take(padded, source_row, axis=0).reshape(peer_count, slot_count, width)
    shared_hidden = activate(normalized_rows, common_expert_gate, common_expert_up)
    piece_width = width // lax.axis_size("tp")
    own_slice = lax.dynamic_slice_in_dim(
        outgoing, lax.axis_index("tp") * piece_width, piece_width, 2
    )
    arrived = lax.all_to_all(own_slice, "ep", split_axis=0, concat_axis=0, tiled=True)
    return (arrived, shared_hidden, target)


def expert_exit(
    arrived,
    shared_hidden,
    target,
    routing_output_weight,
    expert_gate_weight,
    expert_up_weight,
    expert_down_weight,
    common_expert_down,
):
    peer_count, slot_count, piece_width = arrived.shape
    row_count, top_count = routing_output_weight.shape
    out_width = expert_down_weight.shape[2]
    flat_rows = arrived.reshape(-1, piece_width)
    pieces = lax.all_gather(flat_rows, "tp", axis=1, tiled=True)
    gate_cols = expert_gate_weight[0]
    up_cols = expert_up_weight[0]
    pre_gate = jnp.einsum("fd,rd->fr", gate_cols, pieces, preferred_element_type=jnp.float32)
    pre_up = jnp.einsum("fd,rd->fr", up_cols, pieces, preferred_element_type=jnp.float32)
    routed_hidden = (jax.nn.silu(pre_gate) * pre_up).astype(jnp.bfloat16)
    both = lax.all_gather(
        jnp.concatenate([routed_hidden, shared_hidden], axis=1), "tp", axis=0, tiled=True
    )
    pieces = (both[:, : routed_hidden.shape[1]], both[:, routed_hidden.shape[1] :])
    routed_rows = expert_down_weight[0]
    routed_sum = jnp.einsum("fr,fd->rd", pieces[0], routed_rows, preferred_element_type=jnp.float32)
    shared_out = jnp.einsum(
        "fr,fd->rd", pieces[1], common_expert_down, preferred_element_type=jnp.float32
    )
    returned = lax.all_to_all(
        routed_sum.astype(jnp.bfloat16).reshape(peer_count, slot_count, out_width),
        "ep",
        split_axis=0,
        concat_axis=0,
        tiled=True,
    )
    picked = jnp.take(returned.reshape(-1, out_width), target, axis=0).reshape(
        row_count, top_count, out_width
    )
    merged_output = (
        jnp.sum(picked.astype(jnp.float32) * routing_output_weight[:, :, None], axis=1) + shared_out
    )
    return merged_output.astype(jnp.bfloat16)


def on_device(
    receptance,
    key_tensor,
    value_tensor,
    decay_data_input,
    correction_rate_input,
    mixer_output_gate,
    decay_channel_offset,
    head_norm_gain,
    self_key_weight,
    mixer_output_weight,
    second_batch_rows,
    routed_expert_index,
    routing_output_weight,
    expert_norm_gain,
    expert_gate_weight,
    expert_up_weight,
    expert_down_weight,
    common_expert_gate,
    common_expert_up,
    common_expert_down,
):
    arrived, shared_hidden, target = expert_entry(
        second_batch_rows,
        routed_expert_index,
        routing_output_weight,
        expert_norm_gain,
        common_expert_gate,
        common_expert_up,
    )
    arrived, receptance, key_tensor, value_tensor, decay_data_input, correction_rate_input = (
        lax.optimization_barrier(
            (arrived, receptance, key_tensor, value_tensor, decay_data_input, correction_rate_input)
        )
    )
    token_mixer_output = mixer_part(
        receptance,
        key_tensor,
        value_tensor,
        decay_data_input,
        correction_rate_input,
        mixer_output_gate,
        decay_channel_offset,
        head_norm_gain,
        self_key_weight,
        mixer_output_weight,
    )
    expert_out = expert_exit(
        arrived,
        shared_hidden,
        target,
        routing_output_weight,
        expert_gate_weight,
        expert_up_weight,
        expert_down_weight,
        common_expert_down,
    )
    return (token_mixer_output, expert_out)


def solution(mesh):
    in_specs = (
        P("ep", "tp"),
        P("ep", "tp"),
        P("ep", "tp"),
        P("ep", "tp"),
        P("ep", "tp"),
        P("ep", "tp"),
        P("tp"),
        P("tp"),
        P("tp"),
        P("tp", None),
        P("ep", None),
        P("ep", None),
        P("ep", None),
        P(),
        P("ep", "tp", None),
        P("ep", "tp", None),
        P("ep", None, "tp"),
        P("tp", None),
        P("tp", None),
        P(None, "tp"),
    )
    out_specs = (P(("ep", "tp"), None), P("ep", "tp"))
    return jax.shard_map(
        on_device, mesh=mesh, in_specs=in_specs, out_specs=out_specs, check_vma=False
    )
```

profile of v0, /device:TPU:0, one launch (start us, length us, event | category | flops | bytes accessed | tf_op | source)
XLA Modules:
  0.0 244.3 jit_solution(18401035282546436214)
XLA Ops:
  9.3 1.1 reduce-window.6
  10.8 2.4 %scatter_custom_fusion = s32[768]{0:T(1024)S(1)} fusion(s32[512]{0:T(512)S(1)} %bitcast.192, s32[512]{0:T(512)S(1)} %add_select_fusion, s32[]{:T(128)} %constant.328.clone.1), kind=kCustom, calls=%fused_computation.208 | custom fusion | bytes 3076 | tf_op jit(solution)/shard_map/scatter | solution.py:214
  13.3 1.2 fusion.32
  14.6 1.2 fusion.34
  16.7 4.3 %gather_fusion = bf16[768,2048]{1,0:T(8,128)(2,1)} fusion(bf16[129,2048]{1,0:T(8,128)(2,1)S(1)} %concatenate.33, s32[1024]{0:T(1024)S(1)} %pad_clamp_fusion.1), kind=kCustom, calls=%fused_computation | custom fusion | bytes 6294528 | tf_op jit(solution)/shard_map/jit(_take)/gather | solution.py:216
  20.9 2.3 dynamic-slice_select_fusion
  23.2 6.4 %all-to-all-start = ((bf16[8,96,512]{2,1,0:T(8,128)(2,1)}), bf16[8,96,512]{2,1,0:T(8,128)(2,1)S(1)}, u32[]{:S(2)}, u32[]{:S(2)}) async-start(bf16[8,96,512]{2,1,0:T(8,128)(2,1)} %dynamic-slice_select_fusion), calls=%async_computation | async-start | bytes 1572864 | tf_op jit(solution)/shard_map/all_to_all | solution.py:222
  30.5 20.0 %all-to-all-done = bf16[8,96,512]{2,1,0:T(8,128)(2,1)S(1)} async-done(((bf16[8,96,512]{2,1,0:T(8,128)(2,1)}), bf16[8,96,512]{2,1,0:T(8,128)(2,1)S(1)}, u32[]{:S(2)}, u32[]{:S(2)}) %all-to-all-start) | async-done | bytes 786464 | tf_op jit(solution)/shard_map/all_to_all | solution.py:222
  50.7 1.9 copy.246
  52.6 2.3 add_divide_fusion
  54.9 2.2 reshape.842
  57.1 1.4 reshape.885
  58.6 1.6 copy.252
  60.5 2.2 reshape.834
  62.7 2.4 reshape.884
  65.1 2.6 %copy.248 = f32[4,64,8,64]{3,1,2,0:T(8,128)} copy(f32[4,64,8,64]{1,0,3,2:T(4,128)} %reshape.884) | data formatting | bytes 1048576 | tf_op jit(solution)/shard_map/reshape | solution.py:95
  67.7 5.0 %fusion.67 = (f32[4,8,64,64]{3,2,1,0:T(8,128)S(1)}, f32[4,8,64,64]{3,2,1,0:T(8,128)S(1)}, f32[4,8,64,64]{3,2,1,0:T(8,128)S(1)}, f32[4,8,64,64]{3,2,1,0:T(8,128)S(1)}, f32[4,8,64,64]{3,2,1,0:T(8,128)}) fusion(f32[4,64,8,64]{3,2,1,0:T(8,128)} %reshape.842, f32[4,8,64]{2,1,0:T(8,128)S(1)} %add_rsqrt_fusion.1, f32[4,64,8,64]{3,1,2,0:T(8,128)S(1)} %copy.252, ...), kind=kOutput, calls=%fused_computation.114 | convolution fusion | flops 101715968 | bytes 4726784 | tf_op jit(solution)/shard_map/ts,nhsd->nhtd/dot_general | solution.py:105
  72.7 2.3 fusion.1
  82.6 1.6 convolution_subtract_fusion
  84.3 1.6 slice_select_fusion.4
  85.9 2.1 reshape.836
  87.9 2.5 %fusion.8 = f32[4,8,128,64]{3,2,1,0:T(8,128)S(1)} fusion(f32[4,8,64,64]{3,2,1,0:T(8,128)} %get-tuple-element.19, f32[4,8,64,64]{3,2,1,0:T(8,128)} %get-tuple-element.18, bf16[4,8,64,64]{3,1,2,0:T(8,128)(2,1)} %bitcast.178), kind=kOutput, calls=%fused_computation.12 | convolution fusion | flops 100925440 | bytes 2359296 | tf_op jit(solution)/shard_map/nhts,nhsd->nhtd/dot_general | solution.py:47
  90.4 1.1 fusion.129
  94.9 1.7 convolution_subtract_fusion.5
  99.6 1.7 convolution_bitcast_fusion.4
  101.3 2.0 fusion.31
  105.2 2.0 copy.274
  107.3 3.7 %convolution_subtract_fusion.6 = f32[4,8,64,128]{3,2,1,0:T(8,128)} fusion(f32[4,8,64,128]{3,2,1,0:T(8,128)} %copy-done.8, f32[4,8,128,128]{3,2,1,0:T(8,128)} %copy-done.1, f32[4,8,64,64]{3,2,1,0:T(8,128)} %get-tuple-element.16, f32[4,8,64,64]{3,2,1,0:T(8,128)S(1)} %copy-done.7, pred[64,64]{1,0:T(8,128)(4,1)S(1)} %iota_compare_fusion.2), kind=kOutput, calls=%fused_computation.27 | convolution fusion | flops 101318656 | bytes 4722688 | tf_op jit(solution)/shard_map/nhts,nhsd->nhtd/dot_general | solution.py:47
  111.0 9.0 %all-gather.9.cloned.1.call-done = bf16[64,64,128]{2,1,0:T(8,128)(2,1)} async-done(((bf16[8,64,128]{2,1,0:T(8,128)(2,1)}), bf16[64,64,128]{2,1,0:T(8,128)(2,1)}) %all-gather.9.cloned.1.call-update) | async-done | bytes 1048592 | tf_op jit(solution)/shard_map/all_gather | solution.py:144
  120.0 1.2 fusion.27
  121.2 1.2 fusion.26
  122.4 1.2 fusion.25
  123.6 41.5 %all-gather.5.cloned.1.call-done = bf16[768,2048]{1,0:T(8,128)(2,1)} async-done(((bf16[768,512]{1,0:T(8,128)(2,1)}), bf16[768,2048]{1,0:T(8,128)(2,1)}) %all-gather.5.cloned.1.call-update) | async-done | bytes 3145744 | tf_op jit(solution)/shard_map/all_gather | solution.py:240
  165.1 3.3 %convolution_bitcast_fusion.2 = f32[256,768]{0,1:T(8,128)S(1)} fusion(bf16[768,2048]{1,0:T(8,128)(2,1)} %all-gather.5.cloned.1.call-done, bf16[1,256,2048]{2,1,0:T(8,128)(2,1)} %param.34), kind=kOutput, calls=%fused_computation.32 | convolution fusion | flops 805306368 | bytes 4980736 | tf_op jit(solution)/shard_map/fd,rd->fr/dot_general | solution.py:243
  168.5 1.0 fusion.19
  170.7 1.2 fusion.24
  171.9 1.3 fusion.23
  173.2 1.2 fusion.22
  174.4 1.2 fusion.21
  179.6 2.1 copy.273
  181.7 1.1 reshape.837
  183.1 3.2 %convolution_convert_fusion = bf16[256,2048]{1,0:T(8,128)(2,1)} fusion(bf16[512,2048]{1,0:T(8,128)(2,1)S(1)} %copy-done, bf16[256,512]{1,0:T(8,128)(2,1)} %param.25, f32[256,512]{1,0:T(8,128)} %copy.274, bf16[256,512]{1,0:T(8,128)(2,1)S(1)} %copy-done.17, f32[256,512]{1,0:T(8,128)} %copy.273, f32[256,512]{1,0:T(8,128)} %reshape.837, ...), kind=kOutput, calls=%fused_computation.4 | convolution fusion | flops 538574848 | bytes 5769216 | tf_op jit(solution)/shard_map/dot_general | solution.py:174
  186.4 17.0 %all-gather.7.cloned.1.call-done = bf16[1024,896]{0,1:T(8,128)(2,1)} async-done(((bf16[256,896]{0,1:T(8,128)(2,1)}), bf16[1024,896]{0,1:T(8,128)(2,1)}) %all-gather.7.cloned.1.call-update) | async-done | bytes 1835024 | tf_op jit(solution)/shard_map/all_gather | solution.py:246
  203.4 3.5 %fusion.14 = bf16[768,512]{1,0:T(8,128)(2,1)} fusion(bf16[1024,896]{0,1:T(8,128)(2,1)} %all-gather.7.cloned.1.call-done, bf16[1,1024,512]{2,1,0:T(8,128)(2,1)} %param.36), kind=kOutput, calls=%fused_computation.23 | convolution fusion | flops 805699584 | bytes 3407872 | tf_op jit(solution)/shard_map/fr,fd->rd/dot_general | solution.py:251
  207.0 4.6 %all-to-all-start.1 = ((bf16[8,96,512]{2,1,0:T(8,128)(2,1)}), bf16[8,96,512]{2,1,0:T(8,128)(2,1)S(1)}, u32[]{:S(2)}, u32[]{:S(2)}) async-start(bf16[8,96,512]{2,1,0:T(8,128)(2,1)} %bitcast.187), calls=%async_computation.2 | async-start | bytes 1572864 | tf_op jit(solution)/shard_map/all_to_all | solution.py:255
  212.0 20.5 %all-to-all-done.1 = bf16[8,96,512]{2,1,0:T(8,128)(2,1)S(1)} async-done(((bf16[8,96,512]{2,1,0:T(8,128)(2,1)}), bf16[8,96,512]{2,1,0:T(8,128)(2,1)S(1)}, u32[]{:S(2)}, u32[]{:S(2)}) %all-to-all-start.1) | async-done | bytes 786464 | tf_op jit(solution)/shard_map/all_to_all | solution.py:255
  232.5 2.0 gather_fusion.1
  235.5 2.3 fusion.29
  (147 shorter events, 27.1 us)
Async XLA Ops:
  7.2 175.9 %copy-start = (bf16[512,2048]{1,0:T(8,128)(2,1)S(1)}, bf16[512,2048]{1,0:T(8,128)(2,1)}, u32[]{:S(2)}) copy-start(bf16[512,2048]{1,0:T(8,128)(2,1)} %param.29) | copy-start | bytes 6291460
  15.8 0.8 copy-start.12
  20.9 29.6 %copy-start.18 = (bf16[256,512]{1,0:T(8,128)(2,1)S(1)}, bf16[256,512]{1,0:T(8,128)(2,1)}, u32[]{:S(2)}) copy-start(bf16[256,512]{1,0:T(8,128)(2,1)} %param.21) | copy-start | bytes 786436
  20.9 31.7 %copy-start.20 = (f32[512]{0:T(512)S(1)}, f32[512]{0:T(512)}, u32[]{:S(2)}) copy-start(f32[512]{0:T(512)} %param.26) | copy-start | bytes 6148
  23.2 27.3 %all-to-all-start = ((bf16[8,96,512]{2,1,0:T(8,128)(2,1)}), bf16[8,96,512]{2,1,0:T(8,128)(2,1)S(1)}, u32[]{:S(2)}, u32[]{:S(2)}) async-start(bf16[8,96,512]{2,1,0:T(8,128)(2,1)} %dynamic-slice_select_fusion), calls=%async_computation | async-start | bytes 1572864 | tf_op jit(solution)/shard_map/all_to_all | solution.py:222
  29.6 90.4 %all-gather.9.cloned.1.call-start = ((), (), s32[]{:S(2)}) async-start(), calls=%async_computation.6 | async-start | bytes 1179648 | tf_op jit(solution)/shard_map/all_gather | solution.py:144
  50.5 6.6 %copy-start.16 = (bf16[8,96,512]{2,1,0:T(8,128)(2,1)}, bf16[8,96,512]{2,1,0:T(8,128)(2,1)S(1)}, u32[]{:S(2)}) copy-start(bf16[8,96,512]{2,1,0:T(8,128)(2,1)S(1)} %all-to-all-done) | copy-start | bytes 2359300
  72.7 2.3 copy-start.6
  72.7 2.3 copy-start.9
  75.1 9.2 %copy-start.1 = (f32[4,8,128,128]{3,2,1,0:T(8,128)}, f32[4,8,128,128]{3,2,1,0:T(8,128)S(1)}, u32[]{:S(2)}) copy-start(f32[4,8,128,128]{3,2,1,0:T(8,128)S(1)} %fusion.1) | copy-start | bytes 6291460
  90.4 1.6 copy-start.4
  90.4 1.7 copy-start.11
  92.2 1.2 copy-start.10
  92.2 1.5 copy-start.15
  93.7 1.2 copy-start.5
  94.9 1.8 copy-start.8
  96.7 1.1 copy-start.2
  97.0 2.5 %copy-start.22 = (f32[512]{0:T(512)S(1)}, f32[512]{0:T(512)}, u32[]{:S(2)}) copy-start(f32[512]{0:T(512)} %param.28) | copy-start | bytes 6148
  97.0 2.6 %copy-start.13 = (bf16[128,2048]{1,0:T(8,128)(2,1)S(1)}, bf16[128,2048]{1,0:T(8,128)(2,1)}, u32[]{:S(2)}) copy-start(bf16[128,2048]{1,0:T(8,128)(2,1)} %copy-done.12) | copy-start | bytes 1572868
  98.7 66.4 %all-gather.5.cloned.1.call-start = ((), (), s32[]{:S(2)}) async-start(), calls=%async_computation.4 | async-start | bytes 3932160 | tf_op jit(solution)/shard_map/all_gather | solution.py:240
  99.4 104.0 %all-gather.7.cloned.1.call-start = ((), (), s32[]{:S(2)}) async-start(), calls=%async_computation.5 | async-start | bytes 2293760 | tf_op jit(solution)/shard_map/all_gather | solution.py:246
  101.3 6.0 %copy-start.7 = (f32[4,8,64,64]{3,2,1,0:T(8,128)S(1)}, f32[4,8,64,64]{3,2,1,0:T(8,128)}, u32[]{:S(2)}) copy-start(f32[4,8,64,64]{3,2,1,0:T(8,128)} %copy-done.6) | copy-start | bytes 1572868
  123.6 44.9 %copy-start.25 = (bf16[1,256,2048]{2,1,0:T(8,128)(2,1)S(1)}, bf16[1,256,2048]{2,1,0:T(8,128)(2,1)}, u32[]{:S(2)}) copy-start(bf16[1,256,2048]{2,1,0:T(8,128)(2,1)} %param.35) | copy-start | bytes 3145732
  165.1 3.4 %copy-start.24 = (bf16[768,2048]{1,0:T(8,128)(2,1)S(1)}, bf16[768,2048]{1,0:T(8,128)(2,1)}, u32[]{:S(2)}) copy-start(bf16[768,2048]{1,0:T(8,128)(2,1)} %all-gather.5.cloned.1.call-done) | copy-start | bytes 9437188
  169.5 6.1 %copy-start.3 = (f32[4,8,64,128]{3,2,1,0:T(8,128)S(1)}, f32[4,8,64,128]{3,2,1,0:T(8,128)}, u32[]{:S(2)}) copy-start(f32[4,8,64,128]{3,2,1,0:T(8,128)} %copy-done.2) | copy-start | bytes 3145732
  170.4 67.4 %reduce-scatter.2.cloned.1.call-start = ((), (), s32[]{:S(2)}) async-start(), calls=%async_computation.3 | async-start | bytes 1310720 | tf_op jit(solution)/shard_map/reduce_scatter | solution.py:173
  171.9 4.5 %copy-start.14 = (f32[4,8,64,128]{3,2,1,0:T(8,128)S(1)}, f32[4,8,64,128]{3,2,1,0:T(8,128)}, u32[]{:S(2)}) copy-start(f32[4,8,64,128]{3,2,1,0:T(8,128)} %convolution_subtract_fusion.6) | copy-start | bytes 3145732
  179.6 3.5 %copy-start.17 = (bf16[256,512]{1,0:T(8,128)(2,1)S(1)}, bf16[256,512]{1,0:T(8,128)(2,1)}, u32[]{:S(2)}) copy-start(bf16[256,512]{1,0:T(8,128)(2,1)} %param.22) | copy-start | bytes 786436
  179.6 3.5 %copy-start.21 = (f32[512]{0:T(512)S(1)}, f32[512]{0:T(512)}, u32[]{:S(2)}) copy-start(f32[512]{0:T(512)} %param.27) | copy-start | bytes 6148
  186.4 25.3 %copy-start.23 = (f32[128,4]{0,1:T(4,128)S(1)}, f32[128,4]{0,1:T(4,128)}, u32[]{:S(2)}) copy-start(f32[128,4]{0,1:T(4,128)} %param.32) | copy-start | bytes 6148
  186.4 25.5 %copy-start.19 = (s32[128,4]{0,1:T(4,128)S(1)}, s32[128,4]{0,1:T(4,128)}, u32[]{:S(2)}) copy-start(s32[128,4]{0,1:T(4,128)} %param.31) | copy-start | bytes 6148
  207.0 25.6 %all-to-all-start.1 = ((bf16[8,96,512]{2,1,0:T(8,128)(2,1)}), bf16[8,96,512]{2,1,0:T(8,128)(2,1)S(1)}, u32[]{:S(2)}, u32[]{:S(2)}) async-start(bf16[8,96,512]{2,1,0:T(8,128)(2,1)} %bitcast.187), calls=%async_computation.2 | async-start | bytes 1572864 | tf_op jit(solution)/shard_map/all_to_all | solution.py:255
Sparse Core Ops, SparseCore 0:
  98.8 21.1 all-gather.8
  121.8 43.2 all-gather.4
  170.5 32.8 all-gather.6
  206.7 27.9 reduce-scatter.1
where the time goes:
time: 246 us; the launch traced here: 244 us
  waiting for transfers between devices  109 us (44%)
  matrix products  54.7 us (22%)
  local copies, waits for them, and re-layouts  38.5 us (16%)
  other arithmetic  16.2 us (7%)
  between operations  14.6 us (6%)
  starting transfers between devices  11.6 us (5%)
    all_gather x1, waiting for transfers between devices, expert_exit(): pieces = lax.all_gather(flat_rows, 'tp', axis=1, tiled=True)  41.5 us
    dot_general x30, matrix products, product(): jnp.einsum(spec, left, right, precision=PRECISION, preferred_element_type...  32.6 us
    all_to_all x1, waiting for transfers between devices, expert_exit(): lax.all_to_all(routed_sum.astype(jnp.bfloat16).reshape(peer_count, slot_c...  20.5 us
    all_to_all x1, waiting for transfers between devices, expert_entry(): lax.all_to_all(own_slice, 'ep', split_axis=0, concat_axis=0, tiled=True)  20 us
    all_gather x1, waiting for transfers between devices, expert_exit(): lax.all_gather(jnp.concatenate([routed_hidden, shared_hidden], axis=1), '...  17 us
    reshape x6, local copies, waits for them, and re-layouts, by_block(): return matrix.astype(jnp.float32).reshape(block_count, span, head_count,...  12.3 us
    all_gather x1, waiting for transfers between devices, mixer_part(): everything = lax.all_gather(whole.astype(jnp.bfloat16), 'ep')  9.03 us
    all_to_all x1, starting transfers between devices, expert_entry(): lax.all_to_all(own_slice, 'ep', split_axis=0, concat_axis=0, tiled=True)  6.35 us
  transfers between devices with their start and end apart: 6, of which 5 were waited for; matrix products, arithmetic and copies ran while one was open for 17% of the time, Pallas kernels for 0%

commit v1 on v0

--- a/solution.py
+++ b/solution.py
@@ -237,7 +237,8 @@
     row_count, top_count = routing_output_weight.shape
     out_width = expert_down_weight.shape[2]
     flat_rows = arrived.reshape(-1, piece_width)
-    pieces = lax.all_gather(flat_rows, "tp", axis=1, tiled=True)
+    parts = lax.all_gather(flat_rows, "tp", axis=0, tiled=False)
+    pieces = jnp.concatenate(parts, axis=1)
     gate_cols = expert_gate_weight[0]
     up_cols = expert_up_weight[0]
     pre_gate = jnp.einsum("fd,rd->fr", gate_cols, pieces, preferred_element_type=jnp.float32)

time: 246 us -> 250 us (1.016)
  local copies, waits for them, and re-layouts: 38.5 us -> 43.2 us
    all_gather x0 -> x1, local copies, waits for them, and re-layouts: none -> 4.66 us  [expert_exit(): parts = lax.all_gather(flat_rows, 'tp', axis=0, tiled=False)]
  transfers between devices with their start and end apart: 6 -> 6, of which waited for: 5 -> 5; matrix products, arithmetic and copies ran while one was open for 17% -> 16% of each run, Pallas kernels for 0% -> 0%
where the time goes in v1:
time: 250 us; the launch traced here: 249 us
  waiting for transfers between devices  109 us (44%)
  matrix products  54.3 us (22%)
  local copies, waits for them, and re-layouts  43.2 us (17%)
  other arithmetic  16.2 us (6%)
  between operations  14.6 us (6%)
  starting transfers between devices  11.6 us (5%)
    all_gather x1, waiting for transfers between devices, expert_exit(): parts = lax.all_gather(flat_rows, 'tp', axis=0, tiled=False)  41.6 us
    dot_general x30, matrix products, product(): jnp.einsum(spec, left, right, precision=PRECISION, preferred_element_type...  32.6 us
    all_to_all x1, waiting for transfers between devices, expert_exit(): lax.all_to_all(routed_sum.astype(jnp.bfloat16).reshape(peer_count, slot_c...  20.5 us
    all_to_all x1, waiting for transfers between devices, expert_entry(): lax.all_to_all(own_slice, 'ep', split_axis=0, concat_axis=0, tiled=True)  20 us
    all_gather x1, waiting for transfers between devices, expert_exit(): lax.all_gather(jnp.concatenate([routed_hidden, shared_hidden], axis=1), '...  17 us
    reshape x6, local copies, waits for them, and re-layouts, by_block(): return matrix.astype(jnp.float32).reshape(block_count, span, head_count,...  12.2 us
    all_gather x1, waiting for transfers between devices, mixer_part(): everything = lax.all_gather(whole.astype(jnp.bfloat16), 'ep')  9 us
    all_to_all x1, starting transfers between devices, expert_entry(): lax.all_to_all(own_slice, 'ep', split_axis=0, concat_axis=0, tiled=True)  6.35 us
  transfers between devices with their start and end apart: 6, of which 5 were waited for; matrix products, arithmetic and copies ran while one was open for 16% of the time, Pallas kernels for 0%

profile of v1, /device:TPU:0, one launch (start us, length us, event | category | flops | bytes accessed | tf_op | source)
XLA Modules:
  0.0 248.7 jit_solution(16187169213240984861)
XLA Ops:
  9.3 1.1 reduce-window.6
  10.8 2.4 scatter_custom_fusion
  13.3 1.2 fusion.32
  14.6 1.2 fusion.34
  16.7 4.3 %gather_fusion = bf16[768,2048]{1,0:T(8,128)(2,1)} fusion(bf16[129,2048]{1,0:T(8,128)(2,1)S(1)} %concatenate.33, s32[1024]{0:T(1024)S(1)} %pad_clamp_fusion.1), kind=kCustom, calls=%fused_computation | custom fusion | bytes 6294528 | tf_op jit(solution)/shard_map/jit(_take)/gather | solution.py:216
  21.0 2.3 dynamic-slice_select_fusion
  23.3 6.4 %all-to-all-start = ((bf16[8,96,512]{2,1,0:T(8,128)(2,1)}), bf16[8,96,512]{2,1,0:T(8,128)(2,1)S(1)}, u32[]{:S(2)}, u32[]{:S(2)}) async-start(bf16[8,96,512]{2,1,0:T(8,128)(2,1)} %dynamic-slice_select_fusion), calls=%async_computation | async-start | bytes 1572864 | tf_op jit(solution)/shard_map/all_to_all | solution.py:222
  30.6 20.0 %all-to-all-done = bf16[8,96,512]{2,1,0:T(8,128)(2,1)S(1)} async-done(((bf16[8,96,512]{2,1,0:T(8,128)(2,1)}), bf16[8,96,512]{2,1,0:T(8,128)(2,1)S(1)}, u32[]{:S(2)}, u32[]{:S(2)}) %all-to-all-start) | async-done | bytes 786464 | tf_op jit(solution)/shard_map/all_to_all | solution.py:222
  50.7 1.9 copy.339
  52.7 2.3 add_divide_fusion
  55.0 2.3 reshape.846
  57.2 1.4 reshape.889
  58.7 1.6 copy.345
  60.6 2.2 reshape.837
  62.8 2.4 reshape.888
  65.2 2.5 %copy.341 = f32[4,64,8,64]{3,1,2,0:T(8,128)} copy(f32[4,64,8,64]{1,0,3,2:T(4,128)} %reshape.888) | data formatting | bytes 1048576 | tf_op jit(solution)/shard_map/reshape | solution.py:95
  67.8 4.9 %fusion.67 = (f32[4,8,64,64]{3,2,1,0:T(8,128)S(1)}, f32[4,8,64,64]{3,2,1,0:T(8,128)S(1)}, f32[4,8,64,64]{3,2,1,0:T(8,128)S(1)}, f32[4,8,64,64]{3,2,1,0:T(8,128)S(1)}, f32[4,8,64,64]{3,2,1,0:T(8,128)}) fusion(f32[4,64,8,64]{3,2,1,0:T(8,128)} %reshape.846, f32[4,8,64]{2,1,0:T(8,128)S(1)} %add_rsqrt_fusion.1, f32[4,64,8,64]{3,1,2,0:T(8,128)S(1)} %copy.345, ...), kind=kOutput, calls=%fused_computation.114 | convolution fusion | flops 101715968 | bytes 4726784 | tf_op jit(solution)/shard_map/ts,nhsd->nhtd/dot_general | solution.py:105
  72.7 2.3 fusion.1
  82.5 1.7 convolution_subtract_fusion
  84.2 1.6 slice_select_fusion.4
  85.8 2.1 reshape.839
  87.9 2.5 fusion.8
  90.4 1.2 fusion.129
  94.9 1.7 convolution_subtract_fusion.5
  99.4 1.7 convolution_bitcast_fusion.4
  101.2 2.0 fusion.31
  105.1 2.1 copy.367
  107.2 3.7 %convolution_subtract_fusion.6 = f32[4,8,64,128]{3,2,1,0:T(8,128)} fusion(f32[4,8,64,128]{3,2,1,0:T(8,128)} %copy-done.8, f32[4,8,128,128]{3,2,1,0:T(8,128)} %copy-done.1, f32[4,8,64,64]{3,2,1,0:T(8,128)} %get-tuple-element.16, f32[4,8,64,64]{3,2,1,0:T(8,128)S(1)} %copy-done.7, pred[64,64]{1,0:T(8,128)(4,1)S(1)} %iota_compare_fusion.2), kind=kOutput, calls=%fused_computation.27 | convolution fusion | flops 101318656 | bytes 4722688 | tf_op jit(solution)/shard_map/nhts,nhsd->nhtd/dot_general | solution.py:47
  110.9 9.0 %all-gather.9.cloned.1.call-done = bf16[64,64,128]{2,1,0:T(8,128)(2,1)} async-done(((bf16[8,64,128]{2,1,0:T(8,128)(2,1)}), bf16[64,64,128]{2,1,0:T(8,128)(2,1)}) %all-gather.9.cloned.1.call-update) | async-done | bytes 1048592 | tf_op jit(solution)/shard_map/all_gather | solution.py:144
  119.9 1.2 fusion.27
  121.1 1.2 fusion.26
  122.3 1.2 fusion.25
  123.5 41.6 %all-gather.5.cloned.1.call-done = bf16[4,768,512]{2,1,0:T(8,128)(2,1)} async-done(((bf16[1,768,512]{2,1,0:T(8,128)(2,1)}), bf16[4,768,512]{2,1,0:T(8,128)(2,1)}) %all-gather.5.cloned.1.call-update) | async-done | bytes 3145744 | tf_op jit(solution)/shard_map/all_gather | solution.py:240
  165.1 4.7 %copy.370 = bf16[4,768,512]{1,2,0:T(8,128)(2,1)} copy(bf16[4,768,512]{2,1,0:T(8,128)(2,1)} %all-gather.5.cloned.1.call-done) | data formatting | bytes 6291456 | tf_op jit(solution)/shard_map/all_gather | solution.py:240
  169.8 3.1 %convolution_bitcast_fusion.2 = f32[256,768]{0,1:T(8,128)S(1)} fusion(bf16[768,2048]{0,1:T(8,128)(2,1)} %bitcast.182, bf16[1,256,2048]{2,1,0:T(8,128)(2,1)S(1)} %copy-done.25), kind=kOutput, calls=%fused_computation.32 | convolution fusion | flops 805306368 | bytes 4980736 | tf_op jit(solution)/shard_map/fd,rd->fr/dot_general | solution.py:244
  175.1 1.2 fusion.24
  176.3 1.3 fusion.23
  177.6 1.2 fusion.22
  178.8 1.2 fusion.21
  184.1 2.1 copy.366
  186.1 1.1 reshape.840
  187.6 3.2 %convolution_convert_fusion = bf16[256,2048]{1,0:T(8,128)(2,1)} fusion(bf16[512,2048]{1,0:T(8,128)(2,1)S(1)} %copy-done, bf16[256,512]{1,0:T(8,128)(2,1)} %param.25, f32[256,512]{1,0:T(8,128)} %copy.367, bf16[256,512]{1,0:T(8,128)(2,1)S(1)} %copy-done.18, f32[256,512]{1,0:T(8,128)} %copy.366, f32[256,512]{1,0:T(8,128)} %reshape.840, ...), kind=kOutput, calls=%fused_computation.4 | convolution fusion | flops 538574848 | bytes 5769216 | tf_op jit(solution)/shard_map/dot_general | solution.py:174
  190.9 17.0 %all-gather.7.cloned.1.call-done = bf16[1024,896]{0,1:T(8,128)(2,1)} async-done(((bf16[256,896]{0,1:T(8,128)(2,1)}), bf16[1024,896]{0,1:T(8,128)(2,1)}) %all-gather.7.cloned.1.call-update) | async-done | bytes 1835024 | tf_op jit(solution)/shard_map/all_gather | solution.py:247
  207.9 3.6 %fusion.14 = bf16[768,512]{1,0:T(8,128)(2,1)} fusion(bf16[1024,896]{0,1:T(8,128)(2,1)} %all-gather.7.cloned.1.call-done, bf16[1,1024,512]{2,1,0:T(8,128)(2,1)} %param.36), kind=kOutput, calls=%fused_computation.23 | convolution fusion | flops 805699584 | bytes 3407872 | tf_op jit(solution)/shard_map/fr,fd->rd/dot_general | solution.py:252
  211.4 4.6 %all-to-all-start.1 = ((bf16[8,96,512]{2,1,0:T(8,128)(2,1)}), bf16[8,96,512]{2,1,0:T(8,128)(2,1)S(1)}, u32[]{:S(2)}, u32[]{:S(2)}) async-start(bf16[8,96,512]{2,1,0:T(8,128)(2,1)} %bitcast.192), calls=%async_computation.2 | async-start | bytes 1572864 | tf_op jit(solution)/shard_map/all_to_all | solution.py:256
  216.5 20.5 %all-to-all-done.1 = bf16[8,96,512]{2,1,0:T(8,128)(2,1)S(1)} async-done(((bf16[8,96,512]{2,1,0:T(8,128)(2,1)}), bf16[8,96,512]{2,1,0:T(8,128)(2,1)S(1)}, u32[]{:S(2)}, u32[]{:S(2)}) %all-to-all-start.1) | async-done | bytes 786464 | tf_op jit(solution)/shard_map/all_to_all | solution.py:256
  237.0 2.0 gather_fusion.1
  239.9 2.3 fusion.29
  (150 shorter events, 28.1 us)
Async XLA Ops:
  7.2 180.4 %copy-start = (bf16[512,2048]{1,0:T(8,128)(2,1)S(1)}, bf16[512,2048]{1,0:T(8,128)(2,1)}, u32[]{:S(2)}) copy-start(bf16[512,2048]{1,0:T(8,128)(2,1)} %param.29) | copy-start | bytes 6291460
  15.8 0.8 copy-start.12
  21.0 29.6 %copy-start.19 = (bf16[256,512]{1,0:T(8,128)(2,1)S(1)}, bf16[256,512]{1,0:T(8,128)(2,1)}, u32[]{:S(2)}) copy-start(bf16[256,512]{1,0:T(8,128)(2,1)} %param.21) | copy-start | bytes 786436
  21.0 31.7 %copy-start.21 = (f32[512]{0:T(512)S(1)}, f32[512]{0:T(512)}, u32[]{:S(2)}) copy-start(f32[512]{0:T(512)} %param.26) | copy-start | bytes 6148
  23.3 27.3 %all-to-all-start = ((bf16[8,96,512]{2,1,0:T(8,128)(2,1)}), bf16[8,96,512]{2,1,0:T(8,128)(2,1)S(1)}, u32[]{:S(2)}, u32[]{:S(2)}) async-start(bf16[8,96,512]{2,1,0:T(8,128)(2,1)} %dynamic-slice_select_fusion), calls=%async_computation | async-start | bytes 1572864 | tf_op jit(solution)/shard_map/all_to_all | solution.py:222
  29.7 90.2 %all-gather.9.cloned.1.call-start = ((), (), s32[]{:S(2)}) async-start(), calls=%async_computation.6 | async-start | bytes 1179648 | tf_op jit(solution)/shard_map/all_gather | solution.py:144
  50.6 6.6 %copy-start.17 = (bf16[8,96,512]{2,1,0:T(8,128)(2,1)}, bf16[8,96,512]{2,1,0:T(8,128)(2,1)S(1)}, u32[]{:S(2)}) copy-start(bf16[8,96,512]{2,1,0:T(8,128)(2,1)S(1)} %all-to-all-done) | copy-start | bytes 2359300
  72.7 2.3 copy-start.6
  72.7 2.3 copy-start.9
  75.0 9.2 %copy-start.1 = (f32[4,8,128,128]{3,2,1,0:T(8,128)}, f32[4,8,128,128]{3,2,1,0:T(8,128)S(1)}, u32[]{:S(2)}) copy-start(f32[4,8,128,128]{3,2,1,0:T(8,128)S(1)} %fusion.1) | copy-start | bytes 6291460
  90.4 1.6 copy-start.4
  90.4 1.7 copy-start.11
  92.1 1.2 copy-start.10
  92.1 1.5 copy-start.15
  93.6 1.2 copy-start.5
  94.9 1.8 copy-start.8
  96.6 1.0 copy-start.2
  96.9 2.4 copy-start.23
  96.9 2.5 %copy-start.13 = (bf16[128,2048]{1,0:T(8,128)(2,1)S(1)}, bf16[128,2048]{1,0:T(8,128)(2,1)}, u32[]{:S(2)}) copy-start(bf16[128,2048]{1,0:T(8,128)(2,1)} %copy-done.12) | copy-start | bytes 1572868
  98.5 66.6 %all-gather.5.cloned.1.call-start = ((), (), s32[]{:S(2)}) async-start(), calls=%async_computation.4 | async-start | bytes 3932160 | tf_op jit(solution)/shard_map/all_gather | solution.py:240
  99.3 108.6 %all-gather.7.cloned.1.call-start = ((), (), s32[]{:S(2)}) async-start(), calls=%async_computation.5 | async-start | bytes 2293760 | tf_op jit(solution)/shard_map/all_gather | solution.py:247
  101.1 6.0 %copy-start.7 = (f32[4,8,64,64]{3,2,1,0:T(8,128)S(1)}, f32[4,8,64,64]{3,2,1,0:T(8,128)}, u32[]{:S(2)}) copy-start(f32[4,8,64,64]{3,2,1,0:T(8,128)} %copy-done.6) | copy-start | bytes 1572868
  123.5 46.3 %copy-start.25 = (bf16[1,256,2048]{2,1,0:T(8,128)(2,1)S(1)}, bf16[1,256,2048]{2,1,0:T(8,128)(2,1)}, u32[]{:S(2)}) copy-start(bf16[1,256,2048]{2,1,0:T(8,128)(2,1)} %param.34) | copy-start | bytes 3145732
  169.8 3.1 %copy-start.16 = (bf16[4,768,512]{1,2,0:T(8,128)(2,1)S(1)}, bf16[4,768,512]{1,2,0:T(8,128)(2,1)}, u32[]{:S(2)}) copy-start(bf16[4,768,512]{1,2,0:T(8,128)(2,1)} %copy.370) | copy-start | bytes 9437188
  169.8 3.1 %copy-start.26 = (bf16[1,256,2048]{2,1,0:T(8,128)(2,1)S(1)}, bf16[1,256,2048]{2,1,0:T(8,128)(2,1)}, u32[]{:S(2)}) copy-start(bf16[1,256,2048]{2,1,0:T(8,128)(2,1)} %param.35) | copy-start | bytes 3145732
  174.0 6.1 %copy-start.3 = (f32[4,8,64,128]{3,2,1,0:T(8,128)S(1)}, f32[4,8,64,128]{3,2,1,0:T(8,128)}, u32[]{:S(2)}) copy-start(f32[4,8,64,128]{3,2,1,0:T(8,128)} %copy-done.2) | copy-start | bytes 3145732
  174.8 67.4 %reduce-scatter.2.cloned.1.call-start = ((), (), s32[]{:S(2)}) async-start(), calls=%async_computation.3 | async-start | bytes 1310720 | tf_op jit(solution)/shard_map/reduce_scatter | solution.py:173
  176.3 4.5 %copy-start.14 = (f32[4,8,64,128]{3,2,1,0:T(8,128)S(1)}, f32[4,8,64,128]{3,2,1,0:T(8,128)}, u32[]{:S(2)}) copy-start(f32[4,8,64,128]{3,2,1,0:T(8,128)} %convolution_subtract_fusion.6) | copy-start | bytes 3145732
  184.1 3.5 %copy-start.18 = (bf16[256,512]{1,0:T(8,128)(2,1)S(1)}, bf16[256,512]{1,0:T(8,128)(2,1)}, u32[]{:S(2)}) copy-start(bf16[256,512]{1,0:T(8,128)(2,1)} %param.22) | copy-start | bytes 786436
  184.1 3.5 %copy-start.22 = (f32[512]{0:T(512)S(1)}, f32[512]{0:T(512)}, u32[]{:S(2)}) copy-start(f32[512]{0:T(512)} %param.27) | copy-start | bytes 6148
  190.8 25.3 %copy-start.24 = (f32[128,4]{0,1:T(4,128)S(1)}, f32[128,4]{0,1:T(4,128)}, u32[]{:S(2)}) copy-start(f32[128,4]{0,1:T(4,128)} %param.32) | copy-start | bytes 6148
  190.8 25.5 %copy-start.20 = (s32[128,4]{0,1:T(4,128)S(1)}, s32[128,4]{0,1:T(4,128)}, u32[]{:S(2)}) copy-start(s32[128,4]{0,1:T(4,128)} %param.31) | copy-start | bytes 6148
  211.4 25.6 %all-to-all-start.1 = ((bf16[8,96,512]{2,1,0:T(8,128)(2,1)}), bf16[8,96,512]{2,1,0:T(8,128)(2,1)S(1)}, u32[]{:S(2)}, u32[]{:S(2)}) async-start(bf16[8,96,512]{2,1,0:T(8,128)(2,1)} %bitcast.192), calls=%async_computation.2 | async-start | bytes 1572864 | tf_op jit(solution)/shard_map/all_to_all | solution.py:256
Sparse Core Ops, SparseCore 0:
  98.7 21.1 all-gather.8
  121.7 43.3 all-gather.4
  174.9 32.8 all-gather.6
  211.2 27.9 reduce-scatter.1
